TPU v7x, 512 devices: a whole 4x4x16 slice. The times are simulated.
512 devices in a mesh: sp: 128 (over z, x, core), tp: 4 (over y).
Axes of the slice: x: 4, y: 4, z: 16, core: 2. Of those that a mesh axis runs over, the one named last changes fastest.
Arguments:
- tokens: bfloat16 [32768, 2048], P(('sp', 'tp')), may hold values from -40 to 40
- w_query: bfloat16 [2048, 1024], P(None, 'tp'), may hold values from -0.125 to 0.125
- w_key: bfloat16 [2048, 256], P(None, 'tp'), may hold values from -0.125 to 0.125
- w_value: bfloat16 [2048, 256], P(None, 'tp'), may hold values from -0.125 to 0.125
- w_out: bfloat16 [1024, 2048], P('tp'), may hold values from -0.1875 to 0.1875
- cum_gate: float32 [16, 32768], P('tp', 'sp'), may hold values from -4684 to 0, as said below
Outputs:
- layer_out: bfloat16 [32768, 2048], P(('sp', 'tp'))
Inputs may be any that keep to these rules, and one draw needn't show every extreme that they name: `cum_gate`: each head's row does not rise along the positions.
All inputs are finite; a program needn't handle non-finite values.
Results may differ from a plain program's by a relative error of at most 0.012.
Values may be sent and summed in bfloat16 or wider, within the bound.
No kernel may reach another device: no remote copies, remote signals or barrier semaphores. Data moves between devices by JAX's collectives and lax.ppermute only.
A program may use at most 64 MiB of HBM per device.

v0:
```python
import math
import jax
import jax.numpy as jnp
from jax import lax
from jax.sharding import PartitionSpec as P

HD = 64


def sent_to_all(x, axis):
    copies = jnp.broadcast_to(x, (lax.axis_size(axis), *x.shape))
    return lax.all_to_all(copies, axis, split_axis=0, concat_axis=0, tiled=True)


def joined_along(parts, dim):
    dims = list(parts.shape[1:])
    dims[dim] *= parts.shape[0]
    return jnp.moveaxis(parts, 0, dim).reshape(dims)


def collect(x, axis, dim):
    parts = sent_to_all(x, axis)
    return joined_along(parts, dim)


def partner(block, axis, bit):
    count = lax.axis_size(axis)
    route = []
    for low in range(count):
        high = low | 1 << bit
        if high != low and high < count:
            route += [(low, high), (high, low)]
    return lax.ppermute(block, axis, route)


def cut_along(x, dim, peers):
    before, after = (x.shape[:dim], x.shape[dim + 1 :])
    return jnp.moveaxis(x.reshape(*before, peers, -1, *after), dim, 0)


def sent_and_summed(x, axis, dim):
    peers = lax.axis_size(axis)
    parts = lax.all_to_all(cut_along(x, dim, peers), axis, 0, 0, tiled=True)
    return jnp.sum(parts.astype(jnp.float32), axis=0)


def per_device(tokens, w_query, w_key, w_value, w_out, cum_gate):
    pieces = collect(tokens, "tp", 0)
    query_part = jnp.dot(pieces, w_query, preferred_element_type=jnp.float32).astype(jnp.bfloat16)
    key_part = jnp.dot(pieces, w_key, preferred_element_type=jnp.float32).astype(jnp.bfloat16)
    value_part = jnp.dot(pieces, w_value, preferred_element_type=jnp.float32).astype(jnp.bfloat16)
    projected = jnp.concatenate([query_part, key_part, value_part], axis=1)
    row_count = projected.shape[0]
    half_rows = row_count // 2
    heads_local = w_query.shape[1] // HD
    kv_local = w_key.shape[1] // HD
    group_size = heads_local // kv_local
    score_factor = float(HD) ** (-0.5)
    query_flat = projected[:, : heads_local * HD]
    key_values = projected[:, heads_local * HD :]
    first_pos = lax.axis_index("sp") * row_count
    own_pos = first_pos + jnp.arange(row_count, dtype=jnp.int32)
    gate_all = lax.all_gather(cum_gate, "sp", axis=1, tiled=True)
    partner_leading = (lax.axis_size("sp") - 1 - lax.axis_index("sp")) * row_count
    moved = query_flat[half_rows:]
    for bit in range(lax.axis_size("sp").bit_length() - 1):
        moved = partner(moved, "sp", bit)
    partner_start = partner_leading + half_rows
    partner_pos = partner_start + jnp.arange(half_rows, dtype=jnp.int32)
    partner_cum = lax.dynamic_slice_in_dim(gate_all, partner_start, half_rows, 1)
    groups = [
        (query_flat[:half_rows], cum_gate[:, :half_rows], own_pos[:half_rows]),
        (moved, partner_cum, partner_pos),
    ]
    prepared = []
    for query_rows, query_gates, query_pos in groups:
        count = query_rows.shape[0]
        prepared.append(
            (
                query_rows.reshape(count, kv_local, group_size, HD),
                query_gates.reshape(kv_local, group_size, count, 1),
                query_pos,
                jnp.max(query_pos),
            )
        )
    initial = tuple(
        (
            (
                jnp.full((kv_local, group_size, member[2].shape[0]), -1e30, jnp.float32),
                jnp.zeros((kv_local, group_size, member[2].shape[0]), jnp.float32),
                jnp.zeros((kv_local, group_size, member[2].shape[0], HD), jnp.float32),
            )
            for member in prepared
        )
    )
    pieces = lax.all_gather(key_values, "sp", axis=0, tiled=True)
    piece_rows = pieces.shape[0]
    key_block = math.gcd(piece_rows, 1024)

    def one_block(index, hidden_vectors):
        block_start = index * key_block
        slab = lax.dynamic_slice_in_dim(pieces, block_start, key_block, 0)
        key_rows = slab[:, : kv_local * HD].reshape(key_block, kv_local, HD)
        value_rows = slab[:, kv_local * HD :].reshape(key_block, kv_local, HD)
        key_cum = lax.dynamic_slice_in_dim(gate_all, block_start, key_block, 1)
        key_cum = key_cum.reshape(kv_local, group_size, 1, key_block)
        key_pos = block_start + jnp.arange(key_block, dtype=jnp.int32)
        results = []
        for member, state in zip(prepared, hidden_vectors):
            queries, query_cum, query_pos, last_pos = member

            def compute(inner, queries=queries, query_cum=query_cum, query_pos=query_pos):
                top_score, weight_sum, accumulated = inner
                scores = (
                    jnp.einsum(
                        "tkgd,skd->kgts", queries, key_rows, preferred_element_type=jnp.float32
                    )
                    * score_factor
                )
                scores = scores + (query_cum - key_cum)
                scores = jnp.where(key_pos[None, :] <= query_pos[:, None], scores, -jnp.inf)
                new_top = jnp.maximum(top_score, jnp.max(scores, axis=-1))
                weights = jnp.exp(scores - new_top[..., None])
                decay = jnp.exp(top_score - new_top)
                weight_sum = weight_sum * decay + jnp.sum(weights, axis=-1)
                update = jnp.einsum(
                    "kgts,skd->kgtd",
                    weights.astype(jnp.bfloat16),
                    value_rows,
                    preferred_element_type=jnp.float32,
                )
                accumulated = accumulated * decay[..., None] + update
                return (new_top, weight_sum, accumulated)

            def skipped(inner):
                return inner

            results.append(lax.cond(block_start <= last_pos, compute, skipped, state))
        return tuple(results)

    finals = lax.fori_loop(0, piece_rows // key_block, one_block, initial)
    parts = []
    for top_score, weight_sum, accumulated in finals:
        count = weight_sum.shape[2]
        rows = (accumulated / weight_sum[..., None]).astype(jnp.bfloat16)
        parts.append(rows.transpose(2, 0, 1, 3).reshape(count, heads_local * HD))
    attended = jnp.concatenate(parts, axis=0)
    returned = attended[half_rows:]
    for bit in range(lax.axis_size("sp").bit_length() - 1):
        returned = partner(returned, "sp", bit)
    attended = jnp.concatenate([attended[:half_rows], returned], axis=0)
    summed = sent_and_summed(
        jnp.dot(attended, w_out, preferred_element_type=jnp.float32).astype(jnp.bfloat16), "tp", 0
    )
    return summed.astype(jnp.bfloat16)


def solution(mesh):
    placed = (
        P(("sp", "tp"), None),
        P(None, "tp"),
        P(None, "tp"),
        P(None, "tp"),
        P("tp", None),
        P("tp", "sp"),
    )
    return jax.shard_map(
        per_device, mesh=mesh, in_specs=placed, out_specs=P(("sp", "tp"), None), check_vma=False
    )
```

profile of v0, /device:TPU:8, one launch (start us, length us, event | category | flops | bytes accessed | tf_op | source)
XLA Modules:
  0.0 399.6 jit_solution(4949304807565663179)
XLA Ops:
  7.7 18.5 %all_to_all.10 = bf16[4,64,2048]{2,1,0:T(8,128)(2,1)S(1)} all-to-all(bf16[4,64,2048]{2,1,0:T(8,128)(2,1)S(1)} %broadcast_in_dim.27), channel_id=1, replica_groups=mesh['sp'=128,'tp'=4] {'tp'}, dimensions={0} | all-to-all | bytes 2097152 | tf_op jit(solution)/shard_map/all_to_all | solution.py:12
  28.4 1.9 collective-permute-start
  31.5 3.4 collective-permute-start.1
  34.9 2.7 collective-permute-done.1
  37.7 4.9 %collective-permute-start.2 = (bf16[128,256]{0,1:T(8,128)(2,1)S(1)}, bf16[128,256]{0,1:T(8,128)(2,1)S(1)}, u32[]{:S(2)}, u32[]{:S(2)}) collective-permute-start(bf16[128,256]{0,1:T(8,128)(2,1)S(1)} %collective-permute-done.1), channel_id=1, source_target_pairs={{0,16},{16,0},{4,20},{20,4},{8,24},{24,8},{12,28},{28,12},{32,48},... | collective-permute-start | bytes 196616 | tf_op jit(solution)/shard_map/ppermute | solution.py:33
  42.6 2.7 collective-permute-done.2
  45.3 3.8 collective-permute-start.3
  49.1 2.3 collective-permute-done.3
  51.5 5.2 %collective-permute-start.4 = (bf16[128,256]{0,1:T(8,128)(2,1)S(1)}, bf16[128,256]{0,1:T(8,128)(2,1)S(1)}, u32[]{:S(2)}, u32[]{:S(2)}) collective-permute-start(bf16[128,256]{0,1:T(8,128)(2,1)S(1)} %collective-permute-done.3), channel_id=1, source_target_pairs={{0,64},{64,0},{4,68},{68,4},{8,72},{72,8},{12,76},{76,12},{16,80},... | collective-permute-start | bytes 196616 | tf_op jit(solution)/shard_map/ppermute | solution.py:33
  59.0 9.1 %collective-permute-start.5 = (bf16[128,256]{0,1:T(8,128)(2,1)S(1)}, bf16[128,256]{0,1:T(8,128)(2,1)S(1)}, u32[]{:S(2)}, u32[]{:S(2)}) collective-permute-start(bf16[128,256]{0,1:T(8,128)(2,1)S(1)} %collective-permute-done.4), channel_id=1, source_target_pairs={{0,128},{128,0},{4,132},{132,4},{8,136},{136,8},{12,140},{140,12},... | collective-permute-start | bytes 196616 | tf_op jit(solution)/shard_map/ppermute | solution.py:33
  68.1 86.7 %all_gather.7 = f32[4,32768]{1,0:T(4,128)S(1)} all-gather(f32[4,256]{1,0:T(4,128)S(1)} %copy-done.4), channel_id=1, replica_groups=mesh['sp'=128,'tp'=4] {'sp'}, dimensions={1}, use_global_device_ids=true | all-gather | bytes 528384 | tf_op jit(solution)/shard_map/all_gather | solution.py:63
  154.8 7.5 %collective-permute-start.6 = (bf16[128,256]{0,1:T(8,128)(2,1)S(1)}, bf16[128,256]{0,1:T(8,128)(2,1)S(1)}, u32[]{:S(2)}, u32[]{:S(2)}) collective-permute-start(bf16[128,256]{0,1:T(8,128)(2,1)S(1)} %collective-permute-done.5), channel_id=1, source_target_pairs={{0,256},{256,0},{4,260},{260,4},{8,264},{264,8},{12,268},{268,12},... | collective-permute-start | bytes 196616 | tf_op jit(solution)/shard_map/ppermute | solution.py:33
  162.3 13.1 %collective-permute-done.6 = bf16[128,256]{0,1:T(8,128)(2,1)S(1)} collective-permute-done((bf16[128,256]{0,1:T(8,128)(2,1)S(1)}, bf16[128,256]{0,1:T(8,128)(2,1)S(1)}, u32[]{:S(2)}, u32[]{:S(2)}) %collective-permute-start.6) | collective-permute-done | bytes 65568 | tf_op jit(solution)/shard_map/ppermute | solution.py:33
  175.4 9.9 %all-gather.2.cloned.1.call-done = bf16[32768,128]{0,1:T(8,128)(2,1)} async-done(((bf16[256,128]{0,1:T(8,128)(2,1)}), bf16[32768,128]{0,1:T(8,128)(2,1)}) %all-gather.2.cloned.1.call-update) | async-done | bytes 8388624 | tf_op jit(solution)/shard_map/all_gather | solution.py:96
  185.3 134.2 %while.24 = (s32[]{:T(128)}, f32[1,4,128]{2,1,0:T(4,128)S(1)}, f32[1,4,128]{2,1,0:T(4,128)S(1)}, f32[1,4,128,64]{2,3,1,0:T(8,128)S(1)}, f32[1,4,128]{2,1,0:T(4,1...) while((s32[]{:T(128)}, f32[1,4,128]{2,1,0:T(4,128)S(1)}, ...), condition=%wide.region_11.12_spmd.clone, body=%wide.region_2.11_spmd.clone.sunk | while | flops 278270080 | bytes 14961743 | solution.py:141
  193.6 1.8 conditional.7
  197.7 1.8 conditional.7
  206.0 1.8 conditional.7
  214.3 1.8 conditional.7
  218.4 1.8 conditional.7
  222.6 1.8 conditional.7
  226.7 1.8 conditional.7
  230.8 1.8 conditional.7
  239.1 1.8 conditional.7
  247.4 1.8 conditional.7
  251.5 1.8 conditional.7
  255.7 1.8 conditional.7
  263.9 1.8 conditional.7
  272.2 1.8 conditional.7
  280.5 1.8 conditional.7
  288.8 1.8 conditional.7
  297.1 1.8 conditional.7
  305.3 1.8 conditional.7
  313.6 1.8 conditional.7
  319.6 2.2 collective-permute-start.7
  322.7 1.9 collective-permute-start.8
  324.7 4.2 %collective-permute-done.8 = bf16[128,256]{0,1:T(8,128)(2,1)S(1)} collective-permute-done((bf16[128,256]{0,1:T(8,128)(2,1)S(1)}, bf16[128,256]{0,1:T(8,128)(2,1)S(1)}, u32[]{:S(2)}, u32[]{:S(2)}) %collective-permute-start.8) | collective-permute-done | bytes 65568 | tf_op jit(solution)/shard_map/ppermute | solution.py:33
  328.9 3.6 collective-permute-start.9
  332.5 4.1 %collective-permute-done.9 = bf16[128,256]{0,1:T(8,128)(2,1)S(1)} collective-permute-done((bf16[128,256]{0,1:T(8,128)(2,1)S(1)}, bf16[128,256]{0,1:T(8,128)(2,1)S(1)}, u32[]{:S(2)}, u32[]{:S(2)}) %collective-permute-start.9) | collective-permute-done | bytes 65568 | tf_op jit(solution)/shard_map/ppermute | solution.py:33
  336.5 4.2 %collective-permute-start.10 = (bf16[128,256]{0,1:T(8,128)(2,1)S(1)}, bf16[128,256]{0,1:T(8,128)(2,1)S(1)}, u32[]{:S(2)}, u32[]{:S(2)}) collective-permute-start(bf16[128,256]{0,1:T(8,128)(2,1)S(1)} %collective-permute-done.9), channel_id=1, source_target_pairs={{0,32},{32,0},{4,36},{36,4},{8,40},{40,8},{12,44},{44,12},{16,48},... | collective-permute-start | bytes 196616 | tf_op jit(solution)/shard_map/ppermute | solution.py:33
  340.7 2.2 collective-permute-done.10
  343.0 4.5 %collective-permute-start.11 = (bf16[128,256]{0,1:T(8,128)(2,1)S(1)}, bf16[128,256]{0,1:T(8,128)(2,1)S(1)}, u32[]{:S(2)}, u32[]{:S(2)}) collective-permute-start(bf16[128,256]{0,1:T(8,128)(2,1)S(1)} %collective-permute-done.10), channel_id=1, source_target_pairs={{0,64},{64,0},{4,68},{68,4},{8,72},{72,8},{12,76},{76,12},{16,80},... | collective-permute-start | bytes 196616 | tf_op jit(solution)/shard_map/ppermute | solution.py:33
  347.5 2.5 collective-permute-done.11
  350.0 6.7 %collective-permute-start.12 = (bf16[128,256]{0,1:T(8,128)(2,1)S(1)}, bf16[128,256]{0,1:T(8,128)(2,1)S(1)}, u32[]{:S(2)}, u32[]{:S(2)}) collective-permute-start(bf16[128,256]{0,1:T(8,128)(2,1)S(1)} %collective-permute-done.11), channel_id=1, source_target_pairs={{0,128},{128,0},{4,132},{132,4},{8,136},{136,8},{12,140},{140,12},... | collective-permute-start | bytes 196616 | tf_op jit(solution)/shard_map/ppermute | solution.py:33
  356.7 3.4 collective-permute-done.12
  360.1 8.7 %collective-permute-start.13 = (bf16[128,256]{0,1:T(8,128)(2,1)S(1)}, bf16[128,256]{0,1:T(8,128)(2,1)S(1)}, u32[]{:S(2)}, u32[]{:S(2)}) collective-permute-start(bf16[128,256]{0,1:T(8,128)(2,1)S(1)} %collective-permute-done.12), channel_id=1, source_target_pairs={{0,256},{256,0},{4,260},{260,4},{8,264},{264,8},{12,268},{268,12},... | collective-permute-start | bytes 196616 | tf_op jit(solution)/shard_map/ppermute | solution.py:33
  368.8 6.2 %collective-permute-done.13 = bf16[128,256]{0,1:T(8,128)(2,1)S(1)} collective-permute-done((bf16[128,256]{0,1:T(8,128)(2,1)S(1)}, bf16[128,256]{0,1:T(8,128)(2,1)S(1)}, u32[]{:S(2)}, u32[]{:S(2)}) %collective-permute-start.13) | collective-permute-done | bytes 65568 | tf_op jit(solution)/shard_map/ppermute | solution.py:33
  375.5 16.3 %all_to_all.11 = bf16[4,64,2048]{2,1,0:T(8,128)(2,1)S(1)} all-to-all(bf16[4,64,2048]{2,1,0:T(8,128)(2,1)S(1)} %bitcast.112), channel_id=1, replica_groups=mesh['sp'=128,'tp'=4] {'tp'}, dimensions={0} | all-to-all | bytes 2097152 | tf_op jit(solution)/shard_map/all_to_all | solution.py:43
  (473 shorter events, 124.9 us)
Async XLA Ops:
  6.5 368.5 %copy-start = (bf16[256,2048]{1,0:T(8,128)(2,1)S(1)}, bf16[256,2048]{1,0:T(8,128)(2,1)}, u32[]{:S(2)}) copy-start(bf16[256,2048]{1,0:T(8,128)(2,1)} %param.16) | copy-start | bytes 3145732
  6.5 19.7 %copy-start.2 = (bf16[2048,64]{0,1:T(8,128)(2,1)S(1)}, bf16[2048,64]{0,1:T(8,128)(2,1)}, u32[]{:S(2)}) copy-start(bf16[2048,64]{0,1:T(8,128)(2,1)} %param.15) | copy-start | bytes 786436
  6.5 178.7 %all-gather.2.cloned.1.call-start = ((), (), s32[]{:S(2)}) async-start(), calls=%async_computation.2 | async-start | bytes 8454144 | tf_op jit(solution)/shard_map/all_gather | solution.py:96
  6.5 20.1 %copy-start.3 = (bf16[2048,64]{0,1:T(8,128)(2,1)S(1)}, bf16[2048,64]{0,1:T(8,128)(2,1)}, u32[]{:S(2)}) copy-start(bf16[2048,64]{0,1:T(8,128)(2,1)} %param.14) | copy-start | bytes 786436
  7.7 20.1 %copy-start.1 = (bf16[2048,256]{1,0:T(8,128)(2,1)S(1)}, bf16[2048,256]{1,0:T(8,128)(2,1)}, u32[]{:S(2)}) copy-start(bf16[2048,256]{1,0:T(8,128)(2,1)} %param.13) | copy-start | bytes 3145732
  26.7 15.9 %copy-start.4 = (f32[4,256]{1,0:T(4,128)S(1)}, f32[4,256]{1,0:T(4,128)}, u32[]{:S(2)}) copy-start(f32[4,256]{1,0:T(4,128)} %param.17) | copy-start | bytes 12292
  28.4 3.1 collective-permute-start
  31.5 6.1 %collective-permute-start.1 = (bf16[128,256]{0,1:T(8,128)(2,1)S(1)}, bf16[128,256]{0,1:T(8,128)(2,1)S(1)}, u32[]{:S(2)}, u32[]{:S(2)}) collective-permute-start(bf16[128,256]{0,1:T(8,128)(2,1)S(1)} %collective-permute-done), channel_id=1, source_target_pairs={{0,8},{8,0},{4,12},{12,4},{16,24},{24,16},{20,28},{28,20},{32,40},... | collective-permute-start | bytes 196616 | tf_op jit(solution)/shard_map/ppermute | solution.py:33
  37.7 7.7 %collective-permute-start.2 = (bf16[128,256]{0,1:T(8,128)(2,1)S(1)}, bf16[128,256]{0,1:T(8,128)(2,1)S(1)}, u32[]{:S(2)}, u32[]{:S(2)}) collective-permute-start(bf16[128,256]{0,1:T(8,128)(2,1)S(1)} %collective-permute-done.1), channel_id=1, source_target_pairs={{0,16},{16,0},{4,20},{20,4},{8,24},{24,8},{12,28},{28,12},{32,48},... | collective-permute-start | bytes 196616 | tf_op jit(solution)/shard_map/ppermute | solution.py:33
  45.3 6.1 %collective-permute-start.3 = (bf16[128,256]{0,1:T(8,128)(2,1)S(1)}, bf16[128,256]{0,1:T(8,128)(2,1)S(1)}, u32[]{:S(2)}, u32[]{:S(2)}) collective-permute-start(bf16[128,256]{0,1:T(8,128)(2,1)S(1)} %collective-permute-done.2), channel_id=1, source_target_pairs={{0,32},{32,0},{4,36},{36,4},{8,40},{40,8},{12,44},{44,12},{16,48},... | collective-permute-start | bytes 196616 | tf_op jit(solution)/shard_map/ppermute | solution.py:33
  51.5 7.6 %collective-permute-start.4 = (bf16[128,256]{0,1:T(8,128)(2,1)S(1)}, bf16[128,256]{0,1:T(8,128)(2,1)S(1)}, u32[]{:S(2)}, u32[]{:S(2)}) collective-permute-start(bf16[128,256]{0,1:T(8,128)(2,1)S(1)} %collective-permute-done.3), channel_id=1, source_target_pairs={{0,64},{64,0},{4,68},{68,4},{8,72},{72,8},{12,76},{76,12},{16,80},... | collective-permute-start | bytes 196616 | tf_op jit(solution)/shard_map/ppermute | solution.py:33
  59.0 95.8 %collective-permute-start.5 = (bf16[128,256]{0,1:T(8,128)(2,1)S(1)}, bf16[128,256]{0,1:T(8,128)(2,1)S(1)}, u32[]{:S(2)}, u32[]{:S(2)}) collective-permute-start(bf16[128,256]{0,1:T(8,128)(2,1)S(1)} %collective-permute-done.4), channel_id=1, source_target_pairs={{0,128},{128,0},{4,132},{132,4},{8,136},{136,8},{12,140},{140,12},... | collective-permute-start | bytes 196616 | tf_op jit(solution)/shard_map/ppermute | solution.py:33
  154.8 20.5 %collective-permute-start.6 = (bf16[128,256]{0,1:T(8,128)(2,1)S(1)}, bf16[128,256]{0,1:T(8,128)(2,1)S(1)}, u32[]{:S(2)}, u32[]{:S(2)}) collective-permute-start(bf16[128,256]{0,1:T(8,128)(2,1)S(1)} %collective-permute-done.5), channel_id=1, source_target_pairs={{0,256},{256,0},{4,260},{260,4},{8,264},{264,8},{12,268},{268,12},... | collective-permute-start | bytes 196616 | tf_op jit(solution)/shard_map/ppermute | solution.py:33
  319.6 3.1 collective-permute-start.7
  322.7 6.1 %collective-permute-start.8 = (bf16[128,256]{0,1:T(8,128)(2,1)S(1)}, bf16[128,256]{0,1:T(8,128)(2,1)S(1)}, u32[]{:S(2)}, u32[]{:S(2)}) collective-permute-start(bf16[128,256]{0,1:T(8,128)(2,1)S(1)} %collective-permute-done.7), channel_id=1, source_target_pairs={{0,8},{8,0},{4,12},{12,4},{16,24},{24,16},{20,28},{28,20},{32,40},... | collective-permute-start | bytes 196616 | tf_op jit(solution)/shard_map/ppermute | solution.py:33
  328.9 7.7 %collective-permute-start.9 = (bf16[128,256]{0,1:T(8,128)(2,1)S(1)}, bf16[128,256]{0,1:T(8,128)(2,1)S(1)}, u32[]{:S(2)}, u32[]{:S(2)}) collective-permute-start(bf16[128,256]{0,1:T(8,128)(2,1)S(1)} %collective-permute-done.8), channel_id=1, source_target_pairs={{0,16},{16,0},{4,20},{20,4},{8,24},{24,8},{12,28},{28,12},{32,48},... | collective-permute-start | bytes 196616 | tf_op jit(solution)/shard_map/ppermute | solution.py:33
  336.5 6.4 %collective-permute-start.10 = (bf16[128,256]{0,1:T(8,128)(2,1)S(1)}, bf16[128,256]{0,1:T(8,128)(2,1)S(1)}, u32[]{:S(2)}, u32[]{:S(2)}) collective-permute-start(bf16[128,256]{0,1:T(8,128)(2,1)S(1)} %collective-permute-done.9), channel_id=1, source_target_pairs={{0,32},{32,0},{4,36},{36,4},{8,40},{40,8},{12,44},{44,12},{16,48},... | collective-permute-start | bytes 196616 | tf_op jit(solution)/shard_map/ppermute | solution.py:33
  343.0 7.0 %collective-permute-start.11 = (bf16[128,256]{0,1:T(8,128)(2,1)S(1)}, bf16[128,256]{0,1:T(8,128)(2,1)S(1)}, u32[]{:S(2)}, u32[]{:S(2)}) collective-permute-start(bf16[128,256]{0,1:T(8,128)(2,1)S(1)} %collective-permute-done.10), channel_id=1, source_target_pairs={{0,64},{64,0},{4,68},{68,4},{8,72},{72,8},{12,76},{76,12},{16,80},... | collective-permute-start | bytes 196616 | tf_op jit(solution)/shard_map/ppermute | solution.py:33
  350.0 10.1 %collective-permute-start.12 = (bf16[128,256]{0,1:T(8,128)(2,1)S(1)}, bf16[128,256]{0,1:T(8,128)(2,1)S(1)}, u32[]{:S(2)}, u32[]{:S(2)}) collective-permute-start(bf16[128,256]{0,1:T(8,128)(2,1)S(1)} %collective-permute-done.11), channel_id=1, source_target_pairs={{0,128},{128,0},{4,132},{132,4},{8,136},{136,8},{12,140},{140,12},... | collective-permute-start | bytes 196616 | tf_op jit(solution)/shard_map/ppermute | solution.py:33
  360.1 15.0 %collective-permute-start.13 = (bf16[128,256]{0,1:T(8,128)(2,1)S(1)}, bf16[128,256]{0,1:T(8,128)(2,1)S(1)}, u32[]{:S(2)}, u32[]{:S(2)}) collective-permute-start(bf16[128,256]{0,1:T(8,128)(2,1)S(1)} %collective-permute-done.12), channel_id=1, source_target_pairs={{0,256},{256,0},{4,260},{260,4},{8,264},{264,8},{12,268},{268,12},... | collective-permute-start | bytes 196616 | tf_op jit(solution)/shard_map/ppermute | solution.py:33
Sparse Core Ops, SparseCore 0:
  27.9 157.3 all-gather.1
where the time goes:
time: 401 us; the launch traced here: 400 us
  blocking collectives  121 us (30%)
  starting transfers between devices  67.5 us (17%)
  waiting for transfers between devices  56.7 us (14%)
  loops' own time  44.4 us (11%)
  matrix products  41.9 us (10%)
  local copies, waits for them, and re-layouts  33.5 us (8%)
  other arithmetic  20.3 us (5%)
  between operations  13.7 us (3%)
    all_gather x1, blocking collectives, per_device(): gate_all = lax.all_gather(cum_gate, 'sp', axis=1, tiled=True)  86.7 us
    ppermute x14, starting transfers between devices, partner(): return lax.ppermute(block, axis, route)  67.5 us
    ppermute x14, waiting for transfers between devices, partner(): return lax.ppermute(block, axis, route)  46.8 us
    another operation x1, loops' own time, per_device(): finals = lax.fori_loop(0, piece_rows // key_block, one_block, initial)  41.9 us
    reshape x32, local copies, waits for them, and re-layouts, one_block(): value_rows = slab[:, kv_local * HD:].reshape(key_block, kv_local, HD)  31.8 us
    dot_general x33, matrix products, compute(): jnp.einsum('tkgd,skd->kgts', queries, key_rows, preferred_element_type=jn...  24.4 us
    all_to_all x1, blocking collectives, sent_to_all(): return lax.all_to_all(copies, axis, split_axis=0, concat_axis=0, tiled=True)  18.5 us
    all_to_all x1, blocking collectives, sent_and_summed(): parts = lax.all_to_all(cut_along(x, dim, peers), axis, 0, 0, tiled=True)  16.3 us
  transfers between devices with their start and end apart: 15, of which 14 were waited for; matrix products, arithmetic and copies ran while one was open for 0% of the time, Pallas kernels for 0%

commit v1 on v0

--- a/solution.py
+++ b/solution.py
@@ -60,7 +60,9 @@
     key_values = projected[:, heads_local * HD :]
     first_pos = lax.axis_index("sp") * row_count
     own_pos = first_pos + jnp.arange(row_count, dtype=jnp.int32)
-    gate_all = lax.all_gather(cum_gate, "sp", axis=1, tiled=True)
+    gate_all = jnp.concatenate(
+        lax.all_to_all(jnp.stack([cum_gate] * lax.axis_size("sp")), "sp", 0, 0), axis=1
+    )
     partner_leading = (lax.axis_size("sp") - 1 - lax.axis_index("sp")) * row_count
     moved = query_flat[half_rows:]
     for bit in range(lax.axis_size("sp").bit_length() - 1):

time: 401 us -> 429 us (1.070)
  the two profiles are of different devices: /device:TPU:8 before, /device:TPU:64 now
where the time goes in v1:
time: 429 us; the launch traced here: 425 us
  waiting for transfers between devices  137 us (32%)
  starting transfers between devices  76.4 us (18%)
  local copies, waits for them, and re-layouts  58 us (14%)
  loops' own time  43.3 us (10%)
  matrix products  42 us (10%)
  blocking collectives  34.3 us (8%)
  other arithmetic  20.3 us (5%)
  between operations  13.7 us (3%)
    all_gather x1, waiting for transfers between devices, per_device(): pieces = lax.all_gather(key_values, 'sp', axis=0, tiled=True)  79.4 us
    ppermute x14, waiting for transfers between devices, partner(): return lax.ppermute(block, axis, route)  57.7 us
    ppermute x14, starting transfers between devices, partner(): return lax.ppermute(block, axis, route)  57.3 us
    another operation x1, loops' own time, per_device(): finals = lax.fori_loop(0, piece_rows // key_block, one_block, initial)  41.4 us
    reshape x32, local copies, waits for them, and re-layouts, one_block(): value_rows = slab[:, kv_local * HD:].reshape(key_block, kv_local, HD)  31.8 us
    dot_general x33, matrix products, compute(): jnp.einsum('tkgd,skd->kgts', queries, key_rows, preferred_element_type=jn...  24.5 us
    reshape x32, local copies, waits for them, and re-layouts, one_block(): key_cum = key_cum.reshape(kv_local, group_size, 1, key_block)  23.2 us
    all_to_all x1, blocking collectives, sent_to_all(): return lax.all_to_all(copies, axis, split_axis=0, concat_axis=0, tiled=True)  19.4 us
  transfers between devices with their start and end apart: 16, of which 15 were waited for; matrix products, arithmetic and copies ran while one was open for 1% of the time, Pallas kernels for 0%

profile of v1, /device:TPU:64, one launch (start us, length us, event | category | flops | bytes accessed | tf_op | source)
XLA Modules:
  0.0 425.2 jit_solution(13639488979500050847)
XLA Ops:
  7.7 19.4 %all_to_all.15 = bf16[4,64,2048]{2,1,0:T(8,128)(2,1)S(1)} all-to-all(bf16[4,64,2048]{2,1,0:T(8,128)(2,1)S(1)} %broadcast_in_dim.27), channel_id=1, replica_groups=mesh['sp'=128,'tp'=4] {'tp'}, dimensions={0} | all-to-all | bytes 2097152 | tf_op jit(solution)/shard_map/all_to_all | solution.py:12
  29.6 19.0 %all-to-all-start.1 = ((f32[128,4,256]{2,1,0:T(4,128)}), f32[128,4,256]{2,1,0:T(4,128)}, u32[]{:S(2)}, u32[]{:S(2)}) async-start(f32[128,4,256]{2,1,0:T(4,128)} %stack.2), calls=%async_computation.1 | async-start | bytes 1048576 | tf_op jit(solution)/shard_map/all_to_all | solution.py:64
  49.1 2.0 collective-permute-start
  52.3 3.4 collective-permute-start.1
  55.7 3.1 collective-permute-done.1
  58.7 5.2 %collective-permute-start.2 = (bf16[128,256]{0,1:T(8,128)(2,1)S(1)}, bf16[128,256]{0,1:T(8,128)(2,1)S(1)}, u32[]{:S(2)}, u32[]{:S(2)}) collective-permute-start(bf16[128,256]{0,1:T(8,128)(2,1)S(1)} %collective-permute-done.1), channel_id=1, source_target_pairs={{0,16},{16,0},{4,20},{20,4},{8,24},{24,8},{12,28},{28,12},{32,48},... | collective-permute-start | bytes 196616 | tf_op jit(solution)/shard_map/ppermute | solution.py:33
  63.9 2.6 collective-permute-done.2
  66.6 3.8 collective-permute-start.3
  70.4 4.3 %collective-permute-done.3 = bf16[128,256]{0,1:T(8,128)(2,1)S(1)} collective-permute-done((bf16[128,256]{0,1:T(8,128)(2,1)S(1)}, bf16[128,256]{0,1:T(8,128)(2,1)S(1)}, u32[]{:S(2)}, u32[]{:S(2)}) %collective-permute-start.3) | collective-permute-done | bytes 65568 | tf_op jit(solution)/shard_map/ppermute | solution.py:33
  74.7 2.7 collective-permute-start.4
  77.4 4.4 %collective-permute-done.4 = bf16[128,256]{0,1:T(8,128)(2,1)S(1)} collective-permute-done((bf16[128,256]{0,1:T(8,128)(2,1)S(1)}, bf16[128,256]{0,1:T(8,128)(2,1)S(1)}, u32[]{:S(2)}, u32[]{:S(2)}) %collective-permute-start.4) | collective-permute-done | bytes 65568 | tf_op jit(solution)/shard_map/ppermute | solution.py:33
  81.8 8.3 %collective-permute-start.5 = (bf16[128,256]{0,1:T(8,128)(2,1)S(1)}, bf16[128,256]{0,1:T(8,128)(2,1)S(1)}, u32[]{:S(2)}, u32[]{:S(2)}) collective-permute-start(bf16[128,256]{0,1:T(8,128)(2,1)S(1)} %collective-permute-done.4), channel_id=1, source_target_pairs={{0,128},{128,0},{4,132},{132,4},{8,136},{136,8},{12,140},{140,12},... | collective-permute-start | bytes 196616 | tf_op jit(solution)/shard_map/ppermute | solution.py:33
  91.4 2.5 collective-permute-done.5
  93.9 10.0 %collective-permute-start.6 = (bf16[128,256]{0,1:T(8,128)(2,1)S(1)}, bf16[128,256]{0,1:T(8,128)(2,1)S(1)}, u32[]{:S(2)}, u32[]{:S(2)}) collective-permute-start(bf16[128,256]{0,1:T(8,128)(2,1)S(1)} %collective-permute-done.5), channel_id=1, source_target_pairs={{0,256},{256,0},{4,260},{260,4},{8,264},{264,8},{12,268},{268,12},... | collective-permute-start | bytes 196616 | tf_op jit(solution)/shard_map/ppermute | solution.py:33
  104.7 5.9 %collective-permute-done.6 = bf16[128,256]{0,1:T(8,128)(2,1)S(1)} collective-permute-done((bf16[128,256]{0,1:T(8,128)(2,1)S(1)}, bf16[128,256]{0,1:T(8,128)(2,1)S(1)}, u32[]{:S(2)}, u32[]{:S(2)}) %collective-permute-start.6) | collective-permute-done | bytes 65568 | tf_op jit(solution)/shard_map/ppermute | solution.py:33
  110.6 79.4 %all-gather.2.cloned.1.call-done = bf16[32768,128]{0,1:T(8,128)(2,1)} async-done(((bf16[256,128]{0,1:T(8,128)(2,1)}), bf16[32768,128]{0,1:T(8,128)(2,1)}) %all-gather.2.cloned.1.call-update) | async-done | bytes 8388624 | tf_op jit(solution)/shard_map/all_gather | solution.py:98
  190.1 156.1 %while.24 = (s32[]{:T(128)}, f32[1,4,128]{2,1,0:T(4,128)S(1)}, f32[1,4,128]{2,1,0:T(4,128)S(1)}, f32[1,4,128,64]{2,3,1,0:T(8,128)S(1)}, f32[1,4,128]{2,1,0:T(4,1...) while((s32[]{:T(128)}, f32[1,4,128]{2,1,0:T(4,128)S(1)}, ...), condition=%wide.region_11.12_spmd.clone, body=%wide.region_2.11_spmd.clone.sunk | while | flops 278270080 | bytes 14961743 | solution.py:143
  226.1 1.8 conditional.7
  230.9 1.8 conditional.7
  235.7 1.8 conditional.7
  240.6 1.8 conditional.7
  245.4 1.8 conditional.7
  250.2 1.8 conditional.7
  255.0 1.8 conditional.7
  259.9 1.8 conditional.7
  264.7 1.8 conditional.7
  269.5 1.8 conditional.7
  274.3 1.8 conditional.7
  279.2 1.8 conditional.7
  284.0 1.8 conditional.7
  288.8 1.8 conditional.7
  293.6 1.8 conditional.7
  303.3 1.8 conditional.7
  332.2 1.8 conditional.7
  346.2 2.2 collective-permute-start.7
  349.4 1.9 collective-permute-start.8
  351.3 4.2 collective-permute-done.8
  355.5 3.2 collective-permute-start.9
  358.7 4.5 %collective-permute-done.9 = bf16[128,256]{0,1:T(8,128)(2,1)S(1)} collective-permute-done((bf16[128,256]{0,1:T(8,128)(2,1)S(1)}, bf16[128,256]{0,1:T(8,128)(2,1)S(1)}, u32[]{:S(2)}, u32[]{:S(2)}) %collective-permute-start.9) | collective-permute-done | bytes 65568 | tf_op jit(solution)/shard_map/ppermute | solution.py:33
  363.2 2.5 collective-permute-start.10
  365.7 3.6 collective-permute-done.10
  369.3 2.2 collective-permute-start.11
  371.6 4.8 %collective-permute-done.11 = bf16[128,256]{0,1:T(8,128)(2,1)S(1)} collective-permute-done((bf16[128,256]{0,1:T(8,128)(2,1)S(1)}, bf16[128,256]{0,1:T(8,128)(2,1)S(1)}, u32[]{:S(2)}, u32[]{:S(2)}) %collective-permute-start.11) | collective-permute-done | bytes 65568 | tf_op jit(solution)/shard_map/ppermute | solution.py:33
  376.4 4.2 collective-permute-start.12
  380.6 6.5 %collective-permute-done.12 = bf16[128,256]{0,1:T(8,128)(2,1)S(1)} collective-permute-done((bf16[128,256]{0,1:T(8,128)(2,1)S(1)}, bf16[128,256]{0,1:T(8,128)(2,1)S(1)}, u32[]{:S(2)}, u32[]{:S(2)}) %collective-permute-start.12) | collective-permute-done | bytes 65568 | tf_op jit(solution)/shard_map/ppermute | solution.py:33
  387.1 5.7 %collective-permute-start.13 = (bf16[128,256]{0,1:T(8,128)(2,1)S(1)}, bf16[128,256]{0,1:T(8,128)(2,1)S(1)}, u32[]{:S(2)}, u32[]{:S(2)}) collective-permute-start(bf16[128,256]{0,1:T(8,128)(2,1)S(1)} %collective-permute-done.12), channel_id=1, source_target_pairs={{0,256},{256,0},{4,260},{260,4},{8,264},{264,8},{12,268},{268,12},... | collective-permute-start | bytes 196616 | tf_op jit(solution)/shard_map/ppermute | solution.py:33
  392.9 9.1 %collective-permute-done.13 = bf16[128,256]{0,1:T(8,128)(2,1)S(1)} collective-permute-done((bf16[128,256]{0,1:T(8,128)(2,1)S(1)}, bf16[128,256]{0,1:T(8,128)(2,1)S(1)}, u32[]{:S(2)}, u32[]{:S(2)}) %collective-permute-start.13) | collective-permute-done | bytes 65568 | tf_op jit(solution)/shard_map/ppermute | solution.py:33
  402.5 15.0 %all_to_all.16 = bf16[4,64,2048]{2,1,0:T(8,128)(2,1)S(1)} all-to-all(bf16[4,64,2048]{2,1,0:T(8,128)(2,1)S(1)} %bitcast.115), channel_id=1, replica_groups=mesh['sp'=128,'tp'=4] {'tp'}, dimensions={0} | all-to-all | bytes 2097152 | tf_op jit(solution)/shard_map/all_to_all | solution.py:43
  (471 shorter events, 151.2 us)
Async XLA Ops:
  6.5 395.5 %copy-start = (bf16[256,2048]{1,0:T(8,128)(2,1)S(1)}, bf16[256,2048]{1,0:T(8,128)(2,1)}, u32[]{:S(2)}) copy-start(bf16[256,2048]{1,0:T(8,128)(2,1)} %param.16) | copy-start | bytes 3145732
  6.5 20.6 %copy-start.2 = (bf16[2048,64]{0,1:T(8,128)(2,1)S(1)}, bf16[2048,64]{0,1:T(8,128)(2,1)}, u32[]{:S(2)}) copy-start(bf16[2048,64]{0,1:T(8,128)(2,1)} %param.15) | copy-start | bytes 786436
  6.5 183.5 %all-gather.2.cloned.1.call-start = ((), (), s32[]{:S(2)}) async-start(), calls=%async_computation.3 | async-start | bytes 8454144 | tf_op jit(solution)/shard_map/all_gather | solution.py:98
  6.5 21.0 %copy-start.3 = (bf16[2048,64]{0,1:T(8,128)(2,1)S(1)}, bf16[2048,64]{0,1:T(8,128)(2,1)}, u32[]{:S(2)}) copy-start(bf16[2048,64]{0,1:T(8,128)(2,1)} %param.14) | copy-start | bytes 786436
  7.7 20.9 %copy-start.4 = (f32[4,256]{1,0:T(4,128)S(1)}, f32[4,256]{1,0:T(4,128)}, u32[]{:S(2)}) copy-start(f32[4,256]{1,0:T(4,128)} %param.17) | copy-start | bytes 12292
  27.1 21.5 %copy-start.1 = (bf16[2048,256]{1,0:T(8,128)(2,1)S(1)}, bf16[2048,256]{1,0:T(8,128)(2,1)}, u32[]{:S(2)}) copy-start(bf16[2048,256]{1,0:T(8,128)(2,1)} %param.13) | copy-start | bytes 3145732
  29.6 74.4 %all-to-all-start.1 = ((f32[128,4,256]{2,1,0:T(4,128)}), f32[128,4,256]{2,1,0:T(4,128)}, u32[]{:S(2)}, u32[]{:S(2)}) async-start(f32[128,4,256]{2,1,0:T(4,128)} %stack.2), calls=%async_computation.1 | async-start | bytes 1048576 | tf_op jit(solution)/shard_map/all_to_all | solution.py:64
  49.1 3.1 collective-permute-start
  52.3 6.5 %collective-permute-start.1 = (bf16[128,256]{0,1:T(8,128)(2,1)S(1)}, bf16[128,256]{0,1:T(8,128)(2,1)S(1)}, u32[]{:S(2)}, u32[]{:S(2)}) collective-permute-start(bf16[128,256]{0,1:T(8,128)(2,1)S(1)} %collective-permute-done), channel_id=1, source_target_pairs={{0,8},{8,0},{4,12},{12,4},{16,24},{24,16},{20,28},{28,20},{32,40},... | collective-permute-start | bytes 196616 | tf_op jit(solution)/shard_map/ppermute | solution.py:33
  58.7 7.8 %collective-permute-start.2 = (bf16[128,256]{0,1:T(8,128)(2,1)S(1)}, bf16[128,256]{0,1:T(8,128)(2,1)S(1)}, u32[]{:S(2)}, u32[]{:S(2)}) collective-permute-start(bf16[128,256]{0,1:T(8,128)(2,1)S(1)} %collective-permute-done.1), channel_id=1, source_target_pairs={{0,16},{16,0},{4,20},{20,4},{8,24},{24,8},{12,28},{28,12},{32,48},... | collective-permute-start | bytes 196616 | tf_op jit(solution)/shard_map/ppermute | solution.py:33
  66.6 8.1 %collective-permute-start.3 = (bf16[128,256]{0,1:T(8,128)(2,1)S(1)}, bf16[128,256]{0,1:T(8,128)(2,1)S(1)}, u32[]{:S(2)}, u32[]{:S(2)}) collective-permute-start(bf16[128,256]{0,1:T(8,128)(2,1)S(1)} %collective-permute-done.2), channel_id=1, source_target_pairs={{0,32},{32,0},{4,36},{36,4},{8,40},{40,8},{12,44},{44,12},{16,48},... | collective-permute-start | bytes 196616 | tf_op jit(solution)/shard_map/ppermute | solution.py:33
  74.7 7.1 %collective-permute-start.4 = (bf16[128,256]{0,1:T(8,128)(2,1)S(1)}, bf16[128,256]{0,1:T(8,128)(2,1)S(1)}, u32[]{:S(2)}, u32[]{:S(2)}) collective-permute-start(bf16[128,256]{0,1:T(8,128)(2,1)S(1)} %collective-permute-done.3), channel_id=1, source_target_pairs={{0,64},{64,0},{4,68},{68,4},{8,72},{72,8},{12,76},{76,12},{16,80},... | collective-permute-start | bytes 196616 | tf_op jit(solution)/shard_map/ppermute | solution.py:33
  81.8 12.1 %collective-permute-start.5 = (bf16[128,256]{0,1:T(8,128)(2,1)S(1)}, bf16[128,256]{0,1:T(8,128)(2,1)S(1)}, u32[]{:S(2)}, u32[]{:S(2)}) collective-permute-start(bf16[128,256]{0,1:T(8,128)(2,1)S(1)} %collective-permute-done.4), channel_id=1, source_target_pairs={{0,128},{128,0},{4,132},{132,4},{8,136},{136,8},{12,140},{140,12},... | collective-permute-start | bytes 196616 | tf_op jit(solution)/shard_map/ppermute | solution.py:33
  93.9 16.6 %collective-permute-start.6 = (bf16[128,256]{0,1:T(8,128)(2,1)S(1)}, bf16[128,256]{0,1:T(8,128)(2,1)S(1)}, u32[]{:S(2)}, u32[]{:S(2)}) collective-permute-start(bf16[128,256]{0,1:T(8,128)(2,1)S(1)} %collective-permute-done.5), channel_id=1, source_target_pairs={{0,256},{256,0},{4,260},{260,4},{8,264},{264,8},{12,268},{268,12},... | collective-permute-start | bytes 196616 | tf_op jit(solution)/shard_map/ppermute | solution.py:33
  346.2 3.1 collective-permute-start.7
  349.4 6.1 %collective-permute-start.8 = (bf16[128,256]{0,1:T(8,128)(2,1)S(1)}, bf16[128,256]{0,1:T(8,128)(2,1)S(1)}, u32[]{:S(2)}, u32[]{:S(2)}) collective-permute-start(bf16[128,256]{0,1:T(8,128)(2,1)S(1)} %collective-permute-done.7), channel_id=1, source_target_pairs={{0,8},{8,0},{4,12},{12,4},{16,24},{24,16},{20,28},{28,20},{32,40},... | collective-permute-start | bytes 196616 | tf_op jit(solution)/shard_map/ppermute | solution.py:33
  355.5 7.7 %collective-permute-start.9 = (bf16[128,256]{0,1:T(8,128)(2,1)S(1)}, bf16[128,256]{0,1:T(8,128)(2,1)S(1)}, u32[]{:S(2)}, u32[]{:S(2)}) collective-permute-start(bf16[128,256]{0,1:T(8,128)(2,1)S(1)} %collective-permute-done.8), channel_id=1, source_target_pairs={{0,16},{16,0},{4,20},{20,4},{8,24},{24,8},{12,28},{28,12},{32,48},... | collective-permute-start | bytes 196616 | tf_op jit(solution)/shard_map/ppermute | solution.py:33
  363.2 6.1 %collective-permute-start.10 = (bf16[128,256]{0,1:T(8,128)(2,1)S(1)}, bf16[128,256]{0,1:T(8,128)(2,1)S(1)}, u32[]{:S(2)}, u32[]{:S(2)}) collective-permute-start(bf16[128,256]{0,1:T(8,128)(2,1)S(1)} %collective-permute-done.9), channel_id=1, source_target_pairs={{0,32},{32,0},{4,36},{36,4},{8,40},{40,8},{12,44},{44,12},{16,48},... | collective-permute-start | bytes 196616 | tf_op jit(solution)/shard_map/ppermute | solution.py:33
  369.3 7.0 %collective-permute-start.11 = (bf16[128,256]{0,1:T(8,128)(2,1)S(1)}, bf16[128,256]{0,1:T(8,128)(2,1)S(1)}, u32[]{:S(2)}, u32[]{:S(2)}) collective-permute-start(bf16[128,256]{0,1:T(8,128)(2,1)S(1)} %collective-permute-done.10), channel_id=1, source_target_pairs={{0,64},{64,0},{4,68},{68,4},{8,72},{72,8},{12,76},{76,12},{16,80},... | collective-permute-start | bytes 196616 | tf_op jit(solution)/shard_map/ppermute | solution.py:33
  376.4 10.8 %collective-permute-start.12 = (bf16[128,256]{0,1:T(8,128)(2,1)S(1)}, bf16[128,256]{0,1:T(8,128)(2,1)S(1)}, u32[]{:S(2)}, u32[]{:S(2)}) collective-permute-start(bf16[128,256]{0,1:T(8,128)(2,1)S(1)} %collective-permute-done.11), channel_id=1, source_target_pairs={{0,128},{128,0},{4,132},{132,4},{8,136},{136,8},{12,140},{140,12},... | collective-permute-start | bytes 196616 | tf_op jit(solution)/shard_map/ppermute | solution.py:33
  387.1 14.9 %collective-permute-start.13 = (bf16[128,256]{0,1:T(8,128)(2,1)S(1)}, bf16[128,256]{0,1:T(8,128)(2,1)S(1)}, u32[]{:S(2)}, u32[]{:S(2)}) collective-permute-start(bf16[128,256]{0,1:T(8,128)(2,1)S(1)} %collective-permute-done.12), channel_id=1, source_target_pairs={{0,256},{256,0},{4,260},{260,4},{8,264},{264,8},{12,268},{268,12},... | collective-permute-start | bytes 196616 | tf_op jit(solution)/shard_map/ppermute | solution.py:33
Sparse Core Ops, SparseCore 0:
  28.8 161.1 all-gather.1
